TPU v7x, 256 devices: a whole 4x4x8 slice. The times are simulated.
256 devices in a mesh: sp: 32 (over z, x), tp: 8 (over y, core).
Axes of the slice: x: 4, y: 4, z: 8, core: 2. Of those that a mesh axis runs over, the one named last changes fastest.
Arguments:
- tokens: bfloat16 [16384, 2048], P(('sp', 'tp')), may hold values from -64 to 64
- query_weight: bfloat16 [2048, 2048], P(None, 'tp'), may hold values from -0.125 to 0.125
- key_weight: bfloat16 [2048, 2048], P(None, 'tp'), may hold values from -0.125 to 0.125
- value_weight: bfloat16 [2048, 2048], P(None, 'tp'), may hold values from -0.125 to 0.125
- gate_weight: bfloat16 [2048, 2048], P(None, 'tp'), may hold values from -0.125 to 0.125
- forget_weight: bfloat16 [2048, 16], replicated, may hold values from -0.125 to 0.125
- forget_bias: float32 [16], replicated, as said below
- out_weight: bfloat16 [2048, 2048], replicated, may hold values from -0.125 to 0.125
Outputs:
- mixed: bfloat16 [16384, 2048], P(('sp', 'tp'))
Inputs may be any that keep to these rules, and one draw needn't show every extreme that they name: `forget_bias`: every head's forget bias is at least 4.
All inputs are finite; a program needn't handle non-finite values.
Results may differ from a plain program's by a relative error of at most 0.015.
The roundings to bfloat16 on the way count: a program that leaves them out, or rounds other values in their place, can miss the bound.
Values may be sent and summed in bfloat16 or wider, within the bound.
No kernel may reach another device: no remote copies, remote signals or barrier semaphores. Data moves between devices by JAX's collectives and lax.ppermute only.
A program may use at most 128 MiB of HBM per device.

v0:
```python
import math
import jax
import jax.numpy as jnp
from jax import lax
from jax.sharding import PartitionSpec as P

HEAD_DIM = 128


def body(
    tokens,
    query_weight,
    key_weight,
    value_weight,
    gate_weight,
    forget_weight,
    forget_bias,
    out_weight,
):
    width = query_weight.shape[1]
    heads_dev = width // HEAD_DIM
    first_head = lax.axis_index("tp") * heads_dev
    piece = lax.all_gather(tokens, "tp", axis=0, tiled=True)
    products = [
        jnp.dot(piece, weight, preferred_element_type=jnp.float32)
        for weight in (query_weight, key_weight, value_weight, gate_weight, forget_weight)
    ]
    joined = jnp.concatenate(products, axis=1)
    rows = joined.shape[0]
    queries = (
        (joined[:, :width] * HEAD_DIM ** (-0.5))
        .astype(jnp.bfloat16)
        .reshape(rows, heads_dev, HEAD_DIM)
    )
    keys = joined[:, width : 2 * width].astype(jnp.bfloat16)
    values = joined[:, 2 * width : 3 * width].astype(jnp.bfloat16)
    gate = jax.nn.sigmoid(joined[:, 3 * width : 4 * width])
    logits = lax.dynamic_slice_in_dim(joined[:, 4 * width :], first_head, heads_dev, 1)
    bias = lax.dynamic_slice_in_dim(forget_bias, first_head, heads_dev, 0)
    forget_log = jax.nn.log_sigmoid(logits + bias).T
    all_logs = lax.all_gather(forget_log, "sp", axis=1, tiled=True)
    cumul = jnp.cumsum(all_logs, axis=1)
    my_start = lax.axis_index("sp") * rows
    last_query = my_start + rows - 1
    cum_query = lax.dynamic_slice_in_dim(cumul, my_start, rows, 1)
    query_pos = my_start + jnp.arange(rows, dtype=jnp.int32)
    paired = jnp.stack([keys, values])

    def absorb(carry, key_blk, value_blk, key_start):
        best, total, accum = carry
        span = key_blk.shape[0]
        scores = jnp.einsum(
            "qhd,khd->hqk",
            queries,
            key_blk.reshape(span, heads_dev, HEAD_DIM),
            preferred_element_type=jnp.float32,
        )
        cum_key = lax.dynamic_slice_in_dim(cumul, jnp.maximum(key_start, 0), span, 1)
        scores = scores + cum_query[:, :, None] - cum_key[:, None, :]
        key_pos = key_start + jnp.arange(span, dtype=jnp.int32)
        valid = (key_pos[None, :] <= query_pos[:, None]) & (key_pos[None, :] >= 0)
        scores = jnp.where(valid[None], scores, -jnp.inf)
        new_best = jnp.maximum(best, jnp.max(scores, axis=-1))
        factor = jnp.exp(best - new_best)
        weights = jnp.exp(scores - new_best[..., None])
        total = total * factor + jnp.sum(weights, axis=-1)
        accum = accum * factor[..., None] + jnp.einsum(
            "hqk,khd->hqd",
            weights.astype(jnp.bfloat16),
            value_blk.reshape(span, heads_dev, HEAD_DIM),
            preferred_element_type=jnp.float32,
        )
        return (new_best, total, accum)

    initial = (
        jnp.full((heads_dev, rows), -1e30, jnp.float32),
        jnp.zeros((heads_dev, rows), jnp.float32),
        jnp.zeros((heads_dev, rows, HEAD_DIM), jnp.float32),
    )
    carry = initial
    piece = lax.all_gather(paired, "sp", axis=1, tiled=True)
    length = piece.shape[1]
    span = math.gcd(length, 512)
    steps = length // span
    key_blocks = piece[0].reshape(steps, span, width)
    value_blocks = piece[1].reshape(steps, span, width)
    offsets = jnp.arange(steps, dtype=jnp.int32) * span

    def one(state, inputs):
        state = lax.cond(
            inputs[2] <= last_query,
            lambda inner: absorb(inner, inputs[0], inputs[1], inputs[2]),
            lambda inner: inner,
            state,
        )
        return (state, None)

    carry, _ = lax.scan(one, carry, (key_blocks, value_blocks, offsets))
    best, total, accum = carry
    heads_out = (accum / total[..., None]).transpose(1, 0, 2).reshape(rows, width)
    attended = (heads_out * gate).astype(jnp.bfloat16)
    own_rows = lax.dynamic_slice_in_dim(out_weight, first_head * HEAD_DIM, width, 0)
    mixed = lax.psum_scatter(
        jnp.dot(attended, own_rows, preferred_element_type=jnp.float32).astype(jnp.bfloat16),
        "tp",
        scatter_dimension=0,
        tiled=True,
    )
    return mixed


def solution(mesh):
    placed = (
        P(("sp", "tp"), None),
        P(None, "tp"),
        P(None, "tp"),
        P(None, "tp"),
        P(None, "tp"),
        P(),
        P(),
        P(),
    )
    return jax.shard_map(
        body, mesh=mesh, in_specs=placed, out_specs=P(("sp", "tp"), None), check_vma=False
    )
```

profile of v0, /device:TPU:2, one launch (start us, length us, event | category | flops | bytes accessed | tf_op | source)
XLA Modules:
  0.0 454.7 jit_solution(7296809608910442630)
XLA Ops:
  6.5 0.7 all-gather.3.cloned.1.call-update
  7.3 32.7 %all-gather.3.cloned.1.call-done = bf16[512,2048]{1,0:T(8,128)(2,1)} async-done(((bf16[64,2048]{1,0:T(8,128)(2,1)}), bf16[512,2048]{1,0:T(8,128)(2,1)}) %all-gather.3.cloned.1.call-update) | async-done | bytes 2097168 | tf_op jit(solution)/shard_map/all_gather | solution.py:23
  40.1 2.7 fusion.12
  42.9 0.7 fusion.13
  43.6 0.9 pad_maximum_fusion
  44.6 0.6 fusion.22
  45.4 43.4 %all_gather.11 = f32[2,16384]{1,0:T(2,128)S(1)} all-gather(f32[2,512]{1,0:T(2,128)S(1)} %fusion.17), channel_id=1, replica_groups=mesh['sp'=32,'tp'=8] {'sp'}, dimensions={1}, use_global_device_ids=true | all-gather | bytes 135168 | tf_op jit(solution)/shard_map/all_gather | solution.py:41
  89.1 0.3 reduce-window.9
  89.7 2.0 fusion.11
  91.9 91.9 %all-gather.5.cloned.1.call-done = bf16[2,16384,256]{2,1,0:T(8,128)(2,1)} async-done(((bf16[2,512,256]{2,1,0:T(8,128)(2,1)}), bf16[2,16384,256]{2,1,0:T(8,128)(2,1)}) %all-gather.5.cloned.1.call-update) | async-done | bytes 16777232 | tf_op jit(solution)/shard_map/all_gather | solution.py:81
  183.8 11.3 %fusion.21 = (bf16[1,16384,256]{2,1,0:T(8,128)(2,1)}, bf16[1,16384,256]{2,1,0:T(8,128)(2,1)}) fusion(bf16[2,16384,256]{2,1,0:T(8,128)(2,1)} %all-gather.5.cloned.1.call-done), kind=kLoop, calls=%fused_computation.44 | loop fusion | bytes 33554432 | tf_op jit(solution)/shard_map/slice | solution.py:86
  195.0 12.0 %copy.17 = bf16[32,512,256]{1,2,0:T(8,128)(2,1)} copy(bf16[32,512,256]{2,1,0:T(8,128)(2,1)} %bitcast.42) | data formatting | bytes 16777216
  207.1 11.9 %copy.19 = bf16[32,512,256]{1,2,0:T(8,128)(2,1)} copy(bf16[32,512,256]{2,1,0:T(8,128)(2,1)} %bitcast.41) | data formatting | bytes 16777216
  219.0 46.5 %while.15 = (s32[]{:T(128)}, f32[2,512]{1,0:T(2,128)S(1)}, f32[2,512]{1,0:T(2,128)S(1)}, f32[2,512,128]{2,1,0:T(8,128)S(1)}, s32[32]{0:T(128)S(1)}, /*index=5*/s...) while((s32[]{:T(128)}, f32[2,512]{1,0:T(2,128)S(1)}, ...), condition=%wide.region_7.8_spmd.clone, body=%wide.region_2.7_spmd.clone.sunk | while | flops 273420288 | bytes 9794895 | solution.py:98
  219.0 0.6 dynamic_slice.51
  220.1 4.8 %conditional.3 = ((f32[2,512]{1,0:T(2,128)S(1)}, f32[2,512]{1,0:T(2,128)S(1)}, f32[2,512,128]{2,1,0:T(8,128)S(1)})) conditional(s32[]{:T(128)} %convert_element_type.43, (f32[2,512]{1,0:T(2,128)S(1)}, f32[2,512]{1,0:T(2,128)S(1)}, f32[2,512,128]{2,1,0:T(8,128)S(1)}) %tuple.43, (s32[]{:T(128)}, s32[]{:T(128)}, bf16[32,512,256]{1,2,0:T(8,128)(2,1)}, ...), branch_computations={%region_3.3_spmd, %region_4.6_spmd} | conditional | flops 273420288 | bytes 9792576 | solution.py:90
  220.1 0.5 iota_add_fusion
  220.7 0.6 broadcast_compare_fusion
  221.2 0.2 compare_and_fusion
  222.1 1.1 constant_dynamic-slice_fusion
  223.2 0.7 fusion.20
  223.9 0.3 fusion.3
  224.2 0.7 convolution_add_fusion
  225.0 0.6 dynamic_slice.51
  226.1 4.9 %conditional.3 = ((f32[2,512]{1,0:T(2,128)S(1)}, f32[2,512]{1,0:T(2,128)S(1)}, f32[2,512,128]{2,1,0:T(8,128)S(1)})) conditional(s32[]{:T(128)} %convert_element_type.43, (f32[2,512]{1,0:T(2,128)S(1)}, f32[2,512]{1,0:T(2,128)S(1)}, f32[2,512,128]{2,1,0:T(8,128)S(1)}) %tuple.43, (s32[]{:T(128)}, s32[]{:T(128)}, bf16[32,512,256]{1,2,0:T(8,128)(2,1)}, ...), branch_computations={%region_3.3_spmd, %region_4.6_spmd} | conditional | flops 273420288 | bytes 9792576 | solution.py:90
  226.1 0.5 iota_add_fusion
  226.7 0.6 broadcast_compare_fusion
  227.2 0.2 compare_and_fusion
  228.1 1.1 constant_dynamic-slice_fusion
  229.2 0.7 fusion.20
  229.9 0.3 fusion.3
  230.2 0.7 convolution_add_fusion
  231.0 0.6 dynamic_slice.51
  232.1 0.6 dynamic_slice.51
  233.3 0.6 dynamic_slice.51
  234.4 0.6 dynamic_slice.51
  235.6 0.6 dynamic_slice.51
  236.7 0.6 dynamic_slice.51
  237.9 0.6 dynamic_slice.51
  239.0 0.6 dynamic_slice.51
  240.2 0.6 dynamic_slice.51
  241.3 0.6 dynamic_slice.51
  242.5 0.6 dynamic_slice.51
  243.6 0.6 dynamic_slice.51
  244.8 0.6 dynamic_slice.51
  245.9 0.6 dynamic_slice.51
  247.1 0.6 dynamic_slice.51
  248.2 0.6 dynamic_slice.51
  249.4 0.6 dynamic_slice.51
  250.5 0.6 dynamic_slice.51
  251.7 0.6 dynamic_slice.51
  252.8 0.6 dynamic_slice.51
  254.0 0.6 dynamic_slice.51
  255.1 0.6 dynamic_slice.51
  256.3 0.6 dynamic_slice.51
  257.4 0.6 dynamic_slice.51
  258.6 0.6 dynamic_slice.51
  259.7 0.6 dynamic_slice.51
  260.9 0.6 dynamic_slice.51
  262.0 0.6 dynamic_slice.51
  263.2 0.6 dynamic_slice.51
  264.3 0.6 dynamic_slice.51
  265.8 4.8 %convolution_convert_fusion = bf16[512,2048]{1,0:T(8,128)(2,1)} fusion(f32[512,256]{0,1:T(8,128)S(1)} %bitcast.45, bf16[512,2048]{1,0:T(8,128)(2,1)} %all-gather.3.cloned.1.call-done, bf16[2048,256]{1,0:T(8,128)(2,1)S(1)} %copy-done, bf16[2048,2048]{1,0:T(8,128)(2,1)} %param.19, s32[]{:T(128)S(6)} %select_n.25), kind=kOutput, calls=%fused_computation.16 | convolution fusion | flops 1075445760 | bytes 6815748 | tf_op jit(solution)/shard_map/dot_general | solution.py:104
  270.6 177.6 %reduce-scatter.2.cloned.1.call-done = bf16[64,2048]{1,0:T(8,128)(2,1)} async-done(((bf16[512,2048]{1,0:T(8,128)(2,1)}), bf16[64,2048]{1,0:T(8,128)(2,1)}) %reduce-scatter.2.cloned.1.call-update) | async-done | bytes 262160 | tf_op jit(solution)/shard_map/reduce_scatter | solution.py:103
  (103 shorter events, 2.1 us)
Async XLA Ops:
  6.5 259.2 %copy-start = (bf16[2048,256]{1,0:T(8,128)(2,1)S(1)}, bf16[2048,256]{1,0:T(8,128)(2,1)}, u32[]{:S(2)}) copy-start(bf16[2048,256]{1,0:T(8,128)(2,1)} %param.16) | copy-start | bytes 3145732
  6.5 33.5 %all-gather.3.cloned.1.call-start = ((), (), s32[]{:S(2)}) async-start(), calls=%async_computation.1 | async-start | bytes 2359296 | tf_op jit(solution)/shard_map/all_gather | solution.py:23
  7.3 176.5 %all-gather.5.cloned.1.call-start = ((), (), s32[]{:S(2)}) async-start(), calls=%async_computation.2 | async-start | bytes 17301504 | tf_op jit(solution)/shard_map/all_gather | solution.py:81
  40.1 2.7 copy-start.1
  40.1 2.8 copy-start.3
  42.9 1.7 copy-start.4
  42.9 1.8 copy-start.2
  44.5 403.7 %reduce-scatter.2.cloned.1.call-start = ((), (), s32[]{:S(2)}) async-start(), calls=%async_computation.3 | async-start | bytes 2359296 | tf_op jit(solution)/shard_map/reduce_scatter | solution.py:103
Sparse Core Ops, SparseCore 0:
  9.2 30.8 all-gather.2
  44.6 139.1 all-gather.4
  270.7 177.4 reduce-scatter.1
where the time goes:
time: 457 us; the launch traced here: 455 us
  waiting for transfers between devices  303 us (66%)
  local copies, waits for them, and re-layouts  56.2 us (12%)
  blocking collectives  43.4 us (9%)
  loops' own time  20.2 us (4%)
  matrix products  13.7 us (3%)
  between operations  13.3 us (3%)
  other arithmetic  4.91 us (1%)
    reduce_scatter x1, waiting for transfers between devices, body(): lax.psum_scatter(jnp.dot(attended, own_rows, preferred_element_type=jnp.f...  178 us
    all_gather x1, waiting for transfers between devices, body(): piece = lax.all_gather(paired, 'sp', axis=1, tiled=True)  91.9 us
    all_gather x1, blocking collectives, body(): all_logs = lax.all_gather(forget_log, 'sp', axis=1, tiled=True)  43.4 us
    all_gather x1, waiting for transfers between devices, body(): piece = lax.all_gather(tokens, 'tp', axis=0, tiled=True)  32.7 us
    unnamed x15, local copies, waits for them, and re-layouts  24.2 us
    dynamic_slice x34, local copies, waits for them, and re-layouts, body(): carry, _ = lax.scan(one, carry, (key_blocks, value_blocks, offsets))  19.9 us
    another operation x1, loops' own time, body(): carry, _ = lax.scan(one, carry, (key_blocks, value_blocks, offsets))  18.5 us
    slice x1, local copies, waits for them, and re-layouts, body(): value_blocks = piece[1].reshape(steps, span, width)  11.3 us
  transfers between devices with their start and end apart: 3, of which 3 were waited for; matrix products, arithmetic and copies ran while one was open for 1% of the time, Pallas kernels for 0%

commit v1 on v0

--- a/solution.py
+++ b/solution.py
@@ -78,7 +78,7 @@
         jnp.zeros((heads_dev, rows, HEAD_DIM), jnp.float32),
     )
     carry = initial
-    piece = lax.all_gather(paired, "sp", axis=1, tiled=True)
+    piece = jnp.concatenate(lax.all_gather(paired, "sp"), axis=1)
     length = piece.shape[1]
     span = math.gcd(length, 512)
     steps = length // span

time: 457 us -> 471 us (1.031)
  waiting for transfers between devices: 303 us -> 310 us
    unnamed x15, local copies, waits for them, and re-layouts: 24.2 us -> 0.38 us
    all_gather x0 -> x1, local copies, waits for them, and re-layouts: none -> 21.3 us  [body(): piece = jnp.concatenate(lax.all_gather(paired, 'sp'), axis=1)]
    another operation x2 -> x3, local copies, waits for them, and re-layouts: 0.1 us -> 11.5 us  [the longest x1 11.4 us: body(): value_blocks = piece[1].reshape(steps, span, width)]
    slice x2 -> x1, local copies, waits for them, and re-layouts: 11.3 us -> 0.01 us  [the longest x1 11.3 us: body(): value_blocks = piece[1].reshape(steps, span, width)]
    reduce_scatter x1, waiting for transfers between devices: 178 us -> 185 us  [body(): lax.psum_scatter(jnp.dot(attended, own_rows, preferred_element_type=jnp.f...]
where the time goes in v1:
time: 471 us; the launch traced here: 469 us
  waiting for transfers between devices  310 us (66%)
  local copies, waits for them, and re-layouts  57.9 us (12%)
  blocking collectives  43.5 us (9%)
  loops' own time  22.8 us (5%)
  matrix products  13.9 us (3%)
  between operations  13.2 us (3%)
  other arithmetic  7.21 us (2%)
    reduce_scatter x1, waiting for transfers between devices, body(): lax.psum_scatter(jnp.dot(attended, own_rows, preferred_element_type=jnp.f...  185 us
    all_gather x1, waiting for transfers between devices, body(): piece = jnp.concatenate(lax.all_gather(paired, 'sp'), axis=1)  92 us
    all_gather x1, blocking collectives, body(): all_logs = lax.all_gather(forget_log, 'sp', axis=1, tiled=True)  43.5 us
    all_gather x1, waiting for transfers between devices, body(): piece = lax.all_gather(tokens, 'tp', axis=0, tiled=True)  32.7 us
    all_gather x1, local copies, waits for them, and re-layouts, body(): piece = jnp.concatenate(lax.all_gather(paired, 'sp'), axis=1)  21.3 us
    dynamic_slice x34, local copies, waits for them, and re-layouts, body(): carry, _ = lax.scan(one, carry, (key_blocks, value_blocks, offsets))  21.2 us
    another operation x1, loops' own time, body(): carry, _ = lax.scan(one, carry, (key_blocks, value_blocks, offsets))  21 us
    another operation x1, local copies, waits for them, and re-layouts, body(): value_blocks = piece[1].reshape(steps, span, width)  11.4 us
  transfers between devices with their start and end apart: 3, of which 3 were waited for; matrix products, arithmetic and copies ran while one was open for 1% of the time, Pallas kernels for 0%

profile of v1, /device:TPU:2, one launch (start us, length us, event | category | flops | bytes accessed | tf_op | source)
XLA Modules:
  0.0 468.7 jit_solution(3085917844232883580)
XLA Ops:
  6.5 0.7 all-gather.4.cloned.1.call-update
  7.3 32.7 %all-gather.4.cloned.1.call-done = bf16[512,2048]{1,0:T(8,128)(2,1)} async-done(((bf16[64,2048]{1,0:T(8,128)(2,1)}), bf16[512,2048]{1,0:T(8,128)(2,1)}) %all-gather.4.cloned.1.call-update) | async-done | bytes 2097168 | tf_op jit(solution)/shard_map/all_gather | solution.py:23
  40.1 2.7 fusion.12
  42.9 0.7 fusion.13
  43.6 0.9 pad_maximum_fusion
  44.6 0.6 fusion.21
  45.4 43.5 %all_gather.15 = f32[2,16384]{1,0:T(2,128)S(1)} all-gather(f32[2,512]{1,0:T(2,128)S(1)} %fusion.17), channel_id=1, replica_groups=mesh['sp'=32,'tp'=8] {'sp'}, dimensions={1}, use_global_device_ids=true | all-gather | bytes 135168 | tf_op jit(solution)/shard_map/all_gather | solution.py:41
  89.2 0.3 reduce-window.9
  89.7 2.0 fusion.11
  91.9 92.0 %all-gather.6.cloned.1.call-done = bf16[64,512,256]{2,1,0:T(8,128)(2,1)} async-done(((bf16[2,512,256]{2,1,0:T(8,128)(2,1)}), bf16[64,512,256]{2,1,0:T(8,128)(2,1)}) %all-gather.6.cloned.1.call-update) | async-done | bytes 16777232 | tf_op jit(solution)/shard_map/all_gather | solution.py:81
  184.0 21.3 %copy.24 = bf16[32,2,512,256]{2,3,0,1:T(8,128)(2,1)} copy(bf16[32,2,512,256]{3,2,1,0:T(8,128)(2,1)} %bitcast.47) | data formatting | bytes 33554432 | tf_op jit(solution)/shard_map/all_gather | solution.py:81
  205.2 11.4 %slice_bitcast_fusion = (bf16[32,512,256]{1,2,0:T(8,128)(2,1)}, bf16[32,512,256]{1,2,0:T(8,128)(2,1)}) fusion(bf16[2,32,512,256]{2,3,1,0:T(8,128)(2,1)} %bitcast.45), kind=kLoop, calls=%fused_computation.16 | loop fusion | bytes 33554432 | tf_op jit(solution)/shard_map/reshape;squeeze | solution.py:86
  216.7 50.7 %while.15 = (s32[]{:T(128)}, f32[2,512]{1,0:T(2,128)S(1)}, f32[2,512]{1,0:T(2,128)S(1)}, f32[2,512,128]{2,1,0:T(8,128)S(1)}, s32[32]{0:T(128)S(1)}, /*index=5*/s...) while((s32[]{:T(128)}, f32[2,512]{1,0:T(2,128)S(1)}, ...), condition=%wide.region_7.8_spmd.clone, body=%wide.region_2.7_spmd.clone.sunk | while | flops 273420288 | bytes 9794895 | solution.py:98
  216.7 0.6 dynamic_slice.51
  218.0 5.1 %conditional.3 = ((f32[2,512]{1,0:T(2,128)S(1)}, f32[2,512]{1,0:T(2,128)S(1)}, f32[2,512,128]{2,1,0:T(8,128)S(1)})) conditional(s32[]{:T(128)} %convert_element_type.43, (f32[2,512]{1,0:T(2,128)S(1)}, f32[2,512]{1,0:T(2,128)S(1)}, f32[2,512,128]{2,1,0:T(8,128)S(1)}) %tuple.44, (s32[]{:T(128)}, s32[]{:T(128)}, bf16[32,512,256]{1,2,0:T(8,128)(2,1)}, ...), branch_computations={%region_3.3_spmd, %region_4.6_spmd} | conditional | flops 273420288 | bytes 9792576 | solution.py:90
  218.0 0.6 iota_add_fusion
  218.6 0.6 broadcast_compare_fusion
  220.2 1.1 constant_dynamic-slice_fusion
  221.3 0.7 fusion.20
  222.0 0.3 fusion.3
  222.3 0.7 convolution_add_fusion
  223.1 0.6 dynamic_slice.51
  224.3 5.1 %conditional.3 = ((f32[2,512]{1,0:T(2,128)S(1)}, f32[2,512]{1,0:T(2,128)S(1)}, f32[2,512,128]{2,1,0:T(8,128)S(1)})) conditional(s32[]{:T(128)} %convert_element_type.43, (f32[2,512]{1,0:T(2,128)S(1)}, f32[2,512]{1,0:T(2,128)S(1)}, f32[2,512,128]{2,1,0:T(8,128)S(1)}) %tuple.44, (s32[]{:T(128)}, s32[]{:T(128)}, bf16[32,512,256]{1,2,0:T(8,128)(2,1)}, ...), branch_computations={%region_3.3_spmd, %region_4.6_spmd} | conditional | flops 273420288 | bytes 9792576 | solution.py:90
  224.3 0.6 iota_add_fusion
  225.0 0.6 broadcast_compare_fusion
  226.5 1.1 constant_dynamic-slice_fusion
  227.6 0.7 fusion.20
  228.3 0.3 fusion.3
  228.7 0.7 convolution_add_fusion
  229.4 0.6 dynamic_slice.51
  230.7 0.6 dynamic_slice.51
  231.9 0.6 dynamic_slice.51
  233.2 0.6 dynamic_slice.51
  234.5 0.6 dynamic_slice.51
  235.7 0.6 dynamic_slice.51
  237.0 0.6 dynamic_slice.51
  238.3 0.6 dynamic_slice.51
  239.6 0.6 dynamic_slice.51
  240.8 0.6 dynamic_slice.51
  242.1 0.6 dynamic_slice.51
  243.4 0.6 dynamic_slice.51
  244.6 0.6 dynamic_slice.51
  245.9 0.6 dynamic_slice.51
  247.2 0.6 dynamic_slice.51
  248.4 0.6 dynamic_slice.51
  249.7 0.6 dynamic_slice.51
  251.0 0.6 dynamic_slice.51
  252.2 0.6 dynamic_slice.51
  253.5 0.6 dynamic_slice.51
  254.8 0.6 dynamic_slice.51
  256.0 0.6 dynamic_slice.51
  257.3 0.6 dynamic_slice.51
  258.6 0.6 dynamic_slice.51
  259.8 0.6 dynamic_slice.51
  261.1 0.6 dynamic_slice.51
  262.4 0.6 dynamic_slice.51
  263.6 0.6 dynamic_slice.51
  264.9 0.6 dynamic_slice.51
  266.2 0.6 dynamic_slice.51
  267.4 1.0 copy.28
  268.4 2.1 broadcast_divide_fusion
  270.5 2.0 copy.29
  272.6 5.0 %convolution_convert_fusion = bf16[512,2048]{1,0:T(8,128)(2,1)} fusion(f32[512,256]{1,0:T(8,128)} %copy.29, bf16[512,2048]{1,0:T(8,128)(2,1)S(1)} %copy-done.2, bf16[2048,256]{1,0:T(8,128)(2,1)S(1)} %copy-done, bf16[2048,2048]{1,0:T(8,128)(2,1)} %param.19, s32[]{:T(128)S(6)} %select_n.25), kind=kOutput, calls=%fused_computation.18 | convolution fusion | flops 1075445760 | bytes 6815748 | tf_op jit(solution)/shard_map/dot_general | solution.py:104
  277.6 184.5 %reduce-scatter.2.cloned.1.call-done = bf16[64,2048]{1,0:T(8,128)(2,1)} async-done(((bf16[512,2048]{1,0:T(8,128)(2,1)}), bf16[64,2048]{1,0:T(8,128)(2,1)}) %reduce-scatter.2.cloned.1.call-update) | async-done | bytes 262160 | tf_op jit(solution)/shard_map/reduce_scatter | solution.py:103
  (105 shorter events, 2.3 us)
Async XLA Ops:
  6.5 266.0 %copy-start = (bf16[2048,256]{1,0:T(8,128)(2,1)S(1)}, bf16[2048,256]{1,0:T(8,128)(2,1)}, u32[]{:S(2)}) copy-start(bf16[2048,256]{1,0:T(8,128)(2,1)} %param.16) | copy-start | bytes 3145732
  6.5 33.5 %all-gather.4.cloned.1.call-start = ((), (), s32[]{:S(2)}) async-start(), calls=%async_computation.1 | async-start | bytes 2359296 | tf_op jit(solution)/shard_map/all_gather | solution.py:23
  7.3 176.7 %all-gather.6.cloned.1.call-start = ((), (), s32[]{:S(2)}) async-start(), calls=%async_computation.3 | async-start | bytes 17301504 | tf_op jit(solution)/shard_map/all_gather | solution.py:81
  40.1 2.7 copy-start.1
  40.1 2.8 copy-start.4
  42.9 1.7 copy-start.5
  42.9 1.7 copy-start.3
  44.4 417.7 %reduce-scatter.2.cloned.1.call-start = ((), (), s32[]{:S(2)}) async-start(), calls=%async_computation.2 | async-start | bytes 2359296 | tf_op jit(solution)/shard_map/reduce_scatter | solution.py:103
  268.4 4.1 copy-start.2
Sparse Core Ops, SparseCore 0:
  9.2 30.8 all-gather.3
  44.6 139.3 all-gather.5
  277.8 184.3 reduce-scatter.1
